TPU v7x, 32 devices: a whole 2x2x4 slice. The times are simulated.
32 devices in a mesh: ep: 8 (over z, x), tp: 4 (over y, core).
Axes of the slice: x: 2, y: 2, z: 4, core: 2. Of those that a mesh axis runs over, the one named last changes fastest.
Arguments:
- queries: bfloat16 [1024, 1536], P('ep', 'tp'), may hold values from -400 to 400
- token_latents: bfloat16 [1024, 512], P('ep'), may hold values from -6 to 6
- key_rotary: bfloat16 [1024, 32], P('ep'), may hold values from -6 to 6
- latent_norm_gain: float32 [512], replicated, may hold values from 0.1 to 1.9
- latent_up_weight: bfloat16 [512, 2048], P(None, 'tp'), may hold values from -0.25 to 0.25
- w_out: bfloat16 [1024, 2048], P('tp'), may hold values from -0.1875 to 0.1875
- tokens_b: bfloat16 [1024, 2048], P('ep'), may hold values from -6 to 6
- moe_gain: float32 [2048], replicated, may hold values from 0.1 to 1.9
- group_logits: float32 [1024, 4], P('ep'), may hold values from -6 to 6
- inner_logits: float32 [1024, 2], P('ep'), may hold values from -6 to 6
- expert_pick: int32 [1024, 2], P('ep'), may hold values from 0 to 7, as said below
- w_gate: bfloat16 [8, 2048, 4096], P('ep', None, 'tp'), may hold values from -0.125 to 0.125
- w_up: bfloat16 [8, 2048, 4096], P('ep', None, 'tp'), may hold values from -0.125 to 0.125
- w_down: bfloat16 [8, 4096, 2048], P('ep', 'tp'), may hold values from -0.09375 to 0.09375
Outputs:
- mixer_out: bfloat16 [1024, 2048], P(('ep', 'tp'))
- expert_out: bfloat16 [1024, 2048], P('ep', 'tp')
Inputs may be any that keep to these rules, and one draw needn't show every extreme that they name: `expert_pick`: each row names two different experts of one group, a group being 2 consecutive experts. Among the 128 rows of one index of ep no expert is named more than 64 times; in every draw some expert is named exactly 64 times by the rows of every index of ep.
All inputs are finite; a program needn't handle non-finite values.
Results may differ from a plain program's by a relative error of at most 0.018.
The roundings to bfloat16 on the way count: a program that leaves them out, or rounds other values in their place, can miss the bound.
Values may be sent and summed in bfloat16 or wider, within the bound.
A program may use at most 64 MiB of HBM per device.

v0:
```python
import jax
import jax.numpy as jnp
from jax import lax
from jax.sharding import PartitionSpec as P

PLAIN_HEAD_SIZE = 64
D_ROPE = 32
VALUE_HEAD_SIZE = 64
SEGMENT = 64


def rotate(values, positions):
    half_size = values.shape[-1] // 2
    frequency = jnp.power(
        10000.0, -jnp.arange(half_size, dtype=jnp.float32) * 2.0 / values.shape[-1]
    )
    angles = positions[:, None] * frequency[None, :]
    if values.ndim == 3:
        angles = angles[:, None, :]
    cosine = jnp.cos(angles)
    sine_part = jnp.sin(angles)
    first_half = values[..., :half_size]
    second_half = values[..., half_size:]
    return jnp.concatenate(
        [
            first_half * cosine - second_half * sine_part,
            second_half * cosine + first_half * sine_part,
        ],
        axis=-1,
    )


def finish_expert(gate_proj, up_proj, w_down, source_count, item_count, model_width):
    hidden = (jax.nn.silu(gate_proj) * up_proj).astype(jnp.bfloat16)
    partial_value = jnp.dot(hidden, w_down[0], preferred_element_type=jnp.float32)
    partial_value = partial_value.reshape(source_count, item_count, model_width)
    return lax.psum_scatter(
        partial_value.astype(jnp.bfloat16), "tp", scatter_dimension=2, tiled=True
    )


def per_device(
    queries,
    token_latents,
    key_rotary,
    latent_norm_gain,
    latent_up_weight,
    w_out,
    tokens_b,
    moe_gain,
    group_logits,
    inner_logits,
    expert_pick,
    w_gate,
    w_up,
    w_down,
):
    row_count = queries.shape[0]
    heads_here = w_out.shape[0] // VALUE_HEAD_SIZE
    offset = lax.axis_index("ep") * row_count
    token_index = offset + jnp.arange(row_count, dtype=jnp.int32)
    positions = token_index.astype(jnp.float32)
    query_heads = queries.reshape(row_count, heads_here, PLAIN_HEAD_SIZE + D_ROPE)
    q_plain = jnp.transpose(query_heads[:, :, :PLAIN_HEAD_SIZE], (1, 0, 2))
    q_turned = rotate(query_heads[:, :, PLAIN_HEAD_SIZE:].astype(jnp.float32), positions).astype(
        jnp.bfloat16
    )
    q_turned = jnp.transpose(q_turned, (1, 0, 2))
    latent = token_latents.astype(jnp.float32)
    normed_latent = (
        latent
        * lax.rsqrt(jnp.mean(latent * latent, axis=-1, keepdims=True) + 1e-06)
        * latent_norm_gain
    ).astype(jnp.bfloat16)
    k_turned = rotate(key_rotary.astype(jnp.float32), positions).astype(jnp.bfloat16)
    query_segment = token_index // SEGMENT
    scale_factor = (PLAIN_HEAD_SIZE + D_ROPE) ** (-0.5)
    own_keys = jnp.dot(normed_latent, latent_up_weight, preferred_element_type=jnp.float32).astype(
        jnp.bfloat16
    )
    shard_part = (
        lax.all_gather(own_keys, "ep", axis=0, tiled=True),
        lax.all_gather(k_turned, "ep", axis=0, tiled=True),
    )
    projected = shard_part[0].reshape(
        shard_part[0].shape[0], heads_here, PLAIN_HEAD_SIZE + VALUE_HEAD_SIZE
    )
    kv_heads = jnp.transpose(projected, (1, 0, 2))
    run_max = jnp.full((heads_here, row_count), -1e30, jnp.float32)
    key_count = kv_heads.shape[1]
    k_plain = kv_heads[:, :, :PLAIN_HEAD_SIZE]
    values = kv_heads[:, :, PLAIN_HEAD_SIZE:]
    scores = jnp.einsum("hqd,hkd->hqk", q_plain, k_plain, preferred_element_type=jnp.float32)
    scores = scores + jnp.einsum(
        "hqd,kd->hqk", q_turned, shard_part[1], preferred_element_type=jnp.float32
    )
    scores = scores * scale_factor
    key_segment = jnp.arange(key_count, dtype=jnp.int32) // SEGMENT
    allowed = query_segment[:, None] >= key_segment[None, :]
    scores = jnp.where(allowed[None], scores, -jnp.inf)
    new_max = jnp.maximum(run_max, jnp.max(scores, axis=-1))
    weights_raw = jnp.exp(scores - new_max[:, :, None])
    denominator = jnp.sum(weights_raw, axis=-1)
    update = jnp.einsum(
        "hqk,hkd->hqd", weights_raw.astype(jnp.bfloat16), values, preferred_element_type=jnp.float32
    )
    finished = (new_max, denominator, update)
    denominator = finished[1]
    attended = (finished[2] / denominator[:, :, None]).astype(jnp.bfloat16)
    attended = jnp.transpose(attended, (1, 0, 2)).reshape(row_count, heads_here * VALUE_HEAD_SIZE)
    mixer_out = lax.psum_scatter(
        jnp.dot(attended, w_out, preferred_element_type=jnp.float32).astype(jnp.bfloat16),
        "tp",
        scatter_dimension=0,
        tiled=True,
    )
    row_total = tokens_b.shape[0]
    model_width = tokens_b.shape[1]
    experts = lax.axis_size("ep")
    capacity = 4 * row_total // experts
    values_f = tokens_b.astype(jnp.float32)
    centered = values_f - jnp.mean(values_f, axis=-1, keepdims=True)
    variance = jnp.mean(centered * centered, axis=-1, keepdims=True)
    normed = (centered * lax.rsqrt(variance + 1e-05) * moe_gain).astype(jnp.bfloat16)
    flat_picks = expert_pick.reshape(-1)
    owner_row = jnp.arange(2 * row_total, dtype=jnp.int32) // 2
    hit_table = (flat_picks[:, None] == jnp.arange(experts, dtype=jnp.int32)[None, :]).astype(
        jnp.int32
    )
    order_in = jnp.sum(jnp.cumsum(hit_table, axis=0) * hit_table, axis=1) - 1
    slot_index = flat_picks * capacity + order_in
    slot_rows = jnp.zeros((experts * capacity,), jnp.int32).at[slot_index].set(owner_row)
    slot_filled = jnp.zeros((experts * capacity,), jnp.bfloat16).at[slot_index].set(1.0)
    outbound = (normed[slot_rows] * slot_filled[:, None]).reshape(experts, capacity, model_width)
    arrived = lax.all_to_all(outbound, "ep", split_axis=0, concat_axis=0, tiled=True)
    source_count = arrived.shape[0]
    item_count = arrived.shape[1]
    flat_rows = arrived.reshape(source_count * item_count, model_width)
    gate_proj = jnp.dot(flat_rows, w_gate[0], preferred_element_type=jnp.float32)
    up_proj = jnp.dot(flat_rows, w_up[0], preferred_element_type=jnp.float32)
    computed = finish_expert(gate_proj, up_proj, w_down, source_count, item_count, model_width)
    returned = lax.all_to_all(computed, "ep", split_axis=0, concat_axis=0, tiled=True)
    flat_back = returned.reshape(experts * capacity, returned.shape[2])
    chosen = flat_back[slot_index].astype(jnp.float32).reshape(row_total, 2, returned.shape[2])
    per_group = experts // group_logits.shape[1]
    home_group = expert_pick[:, 0] // per_group
    own_logit = jnp.sum(
        jnp.where(
            jnp.arange(group_logits.shape[1], dtype=jnp.int32)[None, :] == home_group[:, None],
            group_logits,
            0.0,
        ),
        axis=1,
    )
    group_share = 1.0 / jnp.sum(jnp.exp(group_logits - own_logit[:, None]), axis=1)
    logit_gap = inner_logits[:, 0] - inner_logits[:, 1]
    route_weight = group_share[:, None] * jnp.stack(
        [jax.nn.sigmoid(logit_gap), jax.nn.sigmoid(-logit_gap)], axis=1
    )
    expert_out = jnp.sum(route_weight[:, :, None] * chosen, axis=1).astype(jnp.bfloat16)
    return (mixer_out, expert_out)


def solution(mesh):
    in_specs = (
        P("ep", "tp"),
        P("ep", None),
        P("ep", None),
        P(),
        P(None, "tp"),
        P("tp", None),
        P("ep", None),
        P(),
        P("ep", None),
        P("ep", None),
        P("ep", None),
        P("ep", None, "tp"),
        P("ep", None, "tp"),
        P("ep", "tp", None),
    )
    out_specs = (P(("ep", "tp"), None), P("ep", "tp"))
    return jax.shard_map(
        per_device, mesh=mesh, in_specs=in_specs, out_specs=out_specs, check_vma=False
    )
```

profile of v0, /device:TPU:0, one launch (start us, length us, event | category | flops | bytes accessed | tf_op | source)
XLA Modules:
  0.0 173.0 jit_solution(17782598538728405183)
XLA Ops:
  8.0 0.9 copy.27
  9.2 0.7 broadcast_multiply_fusion.1
  9.9 0.6 reduce-window.6
  10.4 0.2 slice_reduce_fusion
  11.1 1.4 scatter_custom_fusion
  12.5 1.2 convert_reduce_fusion
  13.7 1.3 fusion.19
  15.0 2.2 %scatter_custom_fusion.1 = bf16[512]{0:T(512)(128)(2,1)S(1)} fusion(s32[256]{0:T(256)S(1)} %bitcast.76, bf16[256]{0:T(256)(128)(2,1)S(1)} %broadcast.302, bf16[]{:T(256)} %constant.101.clone.1), kind=kCustom, calls=%fused_computation.93 | custom fusion | bytes 1026 | tf_op jit(solution)/shard_map/scatter | solution.py:133
  17.3 1.4 fusion.21
  18.7 3.3 %gather_fusion = bf16[512,2048]{1,0:T(8,128)(2,1)} fusion(bf16[128,2048]{1,0:T(8,128)(2,1)S(1)} %fusion.21, s32[1024]{0:T(1024)S(1)} %pad_clamp_fusion.1), kind=kCustom, calls=%fused_computation | custom fusion | bytes 4196352 | tf_op jit(solution)/shard_map/gather | solution.py:134
  22.0 3.1 %broadcast_multiply_fusion = bf16[8,64,2048]{2,1,0:T(8,128)(2,1)} fusion(bf16[8,64,2048]{2,1,0:T(8,128)(2,1)} %bitcast.66, bf16[8,64]{1,0:T(8,128)(2,1)S(1)} %mul.207), kind=kLoop, calls=%fused_computation.30 | loop fusion | flops 1048576 | bytes 4195328 | tf_op jit(solution)/shard_map/mul | solution.py:134
  25.2 7.4 %all-to-all-start = ((bf16[8,64,2048]{2,1,0:T(8,128)(2,1)}), bf16[8,64,2048]{2,1,0:T(8,128)(2,1)S(1)}, u32[]{:S(2)}, u32[]{:S(2)}) async-start(bf16[8,64,2048]{2,1,0:T(8,128)(2,1)} %broadcast_multiply_fusion), calls=%async_computation.1 | async-start | bytes 4194304 | tf_op jit(solution)/shard_map/all_to_all | solution.py:135
  32.8 2.0 %convolution_convert_fusion.1 = bf16[128,512]{1,0:T(8,128)(2,1)} fusion(bf16[512,512]{1,0:T(8,128)(2,1)} %param.18, bf16[128,512]{1,0:T(8,128)(2,1)S(1)} %copy-done.1, f32[512]{0:T(512)S(1)} %copy-done.6, f32[128]{0:T(128)S(1)} %add_rsqrt_fusion.1), kind=kOutput, calls=%fused_computation.23 | convolution fusion | flops 67436544 | bytes 788992 | tf_op jit(solution)/shard_map/dot_general | solution.py:78
  34.8 58.2 %all-to-all-done = bf16[8,64,2048]{2,1,0:T(8,128)(2,1)S(1)} async-done(((bf16[8,64,2048]{2,1,0:T(8,128)(2,1)}), bf16[8,64,2048]{2,1,0:T(8,128)(2,1)S(1)}, u32[]{:S(2)}, u32[]{:S(2)}) %all-to-all-start) | async-done | bytes 2097184 | tf_op jit(solution)/shard_map/all_to_all | solution.py:135
  93.0 4.7 %fusion.4 = f32[512,1024]{1,0:T(8,128)S(1)} fusion(bf16[512,2048]{1,0:T(8,128)(2,1)S(1)} %bitcast.69, bf16[1,2048,1024]{2,1,0:T(8,128)(2,1)} %param.25), kind=kOutput, calls=%fused_computation.8 | convolution fusion | flops 2147483648 | bytes 8388608 | tf_op jit(solution)/shard_map/dot_general | solution.py:139
  97.7 2.5 %multiply_convert_fusion = bf16[512,1024]{1,0:T(8,128)(2,1)S(1)} fusion(f32[512,1024]{1,0:T(8,128)S(1)} %fusion.4, bf16[512,2048]{1,0:T(8,128)(2,1)S(1)} %bitcast.70, bf16[1,2048,1024]{2,1,0:T(8,128)(2,1)S(1)} %copy-done.8), kind=kOutput, calls=%fused_computation.15 | convolution fusion | flops 2150629376 | bytes 9437184 | tf_op jit(solution)/shard_map/dot_general | solution.py:140
  100.2 3.7 %fusion.6 = bf16[8,64,2048]{2,1,0:T(8,128)(2,1)} fusion(bf16[8,64,1024]{2,1,0:T(8,128)(2,1)S(1)} %bitcast.79, bf16[1,1024,2048]{2,1,0:T(8,128)(2,1)S(1)} %copy-done.9), kind=kOutput, calls=%fused_computation.10 | convolution fusion | flops 2148532224 | bytes 7340032 | tf_op jit(solution)/shard_map/dot_general | solution.py:35
  104.0 0.7 copy-done.3
  104.6 0.2 copy-done.2
  105.1 26.2 %all_gather.7 = bf16[1024,32]{0,1:T(8,128)(2,1)S(1)} all-gather(bf16[128,32]{0,1:T(8,128)(2,1)S(1)} %pad_maximum_fusion), channel_id=1, replica_groups=mesh['ep'=8,'tp'=4] {'ep'}, dimensions={0}, use_global_device_ids=true | all-gather | bytes 73728 | tf_op jit(solution)/shard_map/all_gather | solution.py:83
  131.6 1.5 copy.31
  133.1 0.5 fusion.24
  133.7 0.5 fusion.48
  134.2 0.3 fusion.11
  134.5 0.5 fusion.18
  135.1 4.8 %all-to-all-start.1 = ((bf16[8,64,512]{2,1,0:T(8,128)(2,1)}), bf16[8,64,512]{2,1,0:T(8,128)(2,1)S(1)}, u32[]{:S(2)}, u32[]{:S(2)}) async-start(bf16[8,64,512]{2,1,0:T(8,128)(2,1)} %reduce-scatter.5.cloned.1.call-done), calls=%async_computation.3 | async-start | bytes 1048576 | tf_op jit(solution)/shard_map/all_to_all | solution.py:142
  139.9 1.1 convolution_convert_fusion
  141.3 12.9 %all-to-all-done.1 = bf16[8,64,512]{2,1,0:T(8,128)(2,1)S(1)} async-done(((bf16[8,64,512]{2,1,0:T(8,128)(2,1)}), bf16[8,64,512]{2,1,0:T(8,128)(2,1)S(1)}, u32[]{:S(2)}, u32[]{:S(2)}) %all-to-all-start.1) | async-done | bytes 524320 | tf_op jit(solution)/shard_map/all_to_all | solution.py:142
  154.1 1.2 gather_fusion.1
  155.3 0.3 reshape.266
  155.6 1.4 multiply_reduce_fusion
  157.0 8.6 %reduce-scatter.3.cloned.1.call-done = bf16[32,2048]{1,0:T(8,128)(2,1)} async-done(((bf16[128,2048]{1,0:T(8,128)(2,1)}), bf16[32,2048]{1,0:T(8,128)(2,1)}) %reduce-scatter.3.cloned.1.call-update) | async-done | bytes 131088 | tf_op jit(solution)/shard_map/reduce_scatter | solution.py:111
  (65 shorter events, 1.9 us)
Async XLA Ops:
  8.0 131.9 %copy-start = (bf16[256,2048]{1,0:T(8,128)(2,1)S(1)}, bf16[256,2048]{1,0:T(8,128)(2,1)}, u32[]{:S(2)}) copy-start(bf16[256,2048]{1,0:T(8,128)(2,1)} %param.19) | copy-start | bytes 3145732
  25.2 7.5 %copy-start.1 = (bf16[128,512]{1,0:T(8,128)(2,1)S(1)}, bf16[128,512]{1,0:T(8,128)(2,1)}, u32[]{:S(2)}) copy-start(bf16[128,512]{1,0:T(8,128)(2,1)} %param.15) | copy-start | bytes 393220
  25.2 7.6 %copy-start.6 = (f32[512]{0:T(512)S(1)}, f32[512]{0:T(512)}, u32[]{:S(2)}) copy-start(f32[512]{0:T(512)} %param.17) | copy-start | bytes 6148
  25.2 67.8 %all-to-all-start = ((bf16[8,64,2048]{2,1,0:T(8,128)(2,1)}), bf16[8,64,2048]{2,1,0:T(8,128)(2,1)S(1)}, u32[]{:S(2)}, u32[]{:S(2)}) async-start(bf16[8,64,2048]{2,1,0:T(8,128)(2,1)} %broadcast_multiply_fusion), calls=%async_computation.1 | async-start | bytes 4194304 | tf_op jit(solution)/shard_map/all_to_all | solution.py:135
  32.6 99.1 %all-gather.2.cloned.1.call-start = ((), (), s32[]{:S(2)}) async-start(), calls=%async_computation.4 | async-start | bytes 1179648 | tf_op jit(solution)/shard_map/all_gather | solution.py:82
  34.8 100.3 %reduce-scatter.5.cloned.1.call-start = ((), (), s32[]{:S(2)}) async-start(), calls=%async_computation.6 | async-start | bytes 2621440 | tf_op jit(solution)/shard_map/reduce_scatter | solution.py:37
  93.0 4.7 %copy-start.8 = (bf16[1,2048,1024]{2,1,0:T(8,128)(2,1)S(1)}, bf16[1,2048,1024]{2,1,0:T(8,128)(2,1)}, u32[]{:S(2)}) copy-start(bf16[1,2048,1024]{2,1,0:T(8,128)(2,1)} %param.26) | copy-start | bytes 12582916
  97.6 2.6 %copy-start.9 = (bf16[1,1024,2048]{2,1,0:T(8,128)(2,1)S(1)}, bf16[1,1024,2048]{2,1,0:T(8,128)(2,1)}, u32[]{:S(2)}) copy-start(bf16[1,1024,2048]{2,1,0:T(8,128)(2,1)} %param.27) | copy-start | bytes 12582916
  103.9 0.7 copy-start.3
  103.9 0.9 copy-start.2
  103.9 27.4 %copy-start.5 = (s32[128,2]{0,1:T(2,128)S(1)}, s32[128,2]{0,1:T(2,128)}, u32[]{:S(2)}) copy-start(s32[128,2]{0,1:T(2,128)} %param.24) | copy-start | bytes 3076
  103.9 27.4 %copy-start.4 = (f32[128,4]{0,1:T(4,128)S(1)}, f32[128,4]{0,1:T(4,128)}, u32[]{:S(2)}) copy-start(f32[128,4]{0,1:T(4,128)} %param.22) | copy-start | bytes 6148
  135.0 6.1 %copy-start.7 = (f32[128,2]{0,1:T(2,128)S(1)}, f32[128,2]{0,1:T(2,128)}, u32[]{:S(2)}) copy-start(f32[128,2]{0,1:T(2,128)} %param.23) | copy-start | bytes 3076
  135.1 19.0 %all-to-all-start.1 = ((bf16[8,64,512]{2,1,0:T(8,128)(2,1)}), bf16[8,64,512]{2,1,0:T(8,128)(2,1)S(1)}, u32[]{:S(2)}, u32[]{:S(2)}) async-start(bf16[8,64,512]{2,1,0:T(8,128)(2,1)} %reduce-scatter.5.cloned.1.call-done), calls=%async_computation.3 | async-start | bytes 1048576 | tf_op jit(solution)/shard_map/all_to_all | solution.py:142
  139.9 25.7 %reduce-scatter.3.cloned.1.call-start = ((), (), s32[]{:S(2)}) async-start(), calls=%async_computation.5 | async-start | bytes 655360 | tf_op jit(solution)/shard_map/reduce_scatter | solution.py:111
Sparse Core Ops, SparseCore 0:
  36.1 57.8 all-gather.1
Sparse Core Ops, SparseCore 1:
  104.1 30.3 reduce-scatter.4
  143.4 22.1 reduce-scatter.2
where the time goes:
time: 174 us; the launch traced here: 173 us
  waiting for transfers between devices  79.7 us (46%)
  blocking collectives  26.2 us (15%)
  between operations  15.8 us (9%)
  matrix products  15.6 us (9%)
  local copies, waits for them, and re-layouts  12.7 us (7%)
  starting transfers between devices  12.3 us (7%)
  other arithmetic  10.8 us (6%)
    all_to_all x1, waiting for transfers between devices, per_device(): lax.all_to_all(outbound, 'ep', split_axis=0, concat_axis=0, tiled=True)  58.2 us
    all_gather x1, blocking collectives, per_device(): lax.all_gather(k_turned, 'ep', axis=0, tiled=True)  26.2 us
    all_to_all x1, waiting for transfers between devices, per_device(): lax.all_to_all(computed, 'ep', split_axis=0, concat_axis=0, tiled=True)  12.9 us
    reduce_scatter x1, waiting for transfers between devices, per_device(): lax.psum_scatter(jnp.dot(attended, w_out, preferred_element_type=jnp.floa...  8.59 us
    all_to_all x1, starting transfers between devices, per_device(): lax.all_to_all(outbound, 'ep', split_axis=0, concat_axis=0, tiled=True)  7.41 us
    all_to_all x1, starting transfers between devices, per_device(): lax.all_to_all(computed, 'ep', split_axis=0, concat_axis=0, tiled=True)  4.77 us
    dot_general x1, matrix products, per_device(): jnp.dot(flat_rows, w_gate[0], preferred_element_type=jnp.float32)  4.66 us
    dot_general x1, matrix products, finish_expert(): jnp.dot(hidden, w_down[0], preferred_element_type=jnp.float32)  3.72 us
  transfers between devices with their start and end apart: 5, of which 3 were waited for; matrix products, arithmetic and copies ran while one was open for 12% of the time, Pallas kernels for 0%

commit v1 on v0

--- a/solution.py
+++ b/solution.py
@@ -1,6 +1,10 @@
+import functools
+
 import jax
 import jax.numpy as jnp
 from jax import lax
+from jax.experimental import pallas as pl
+from jax.experimental.pallas import tpu as pltpu
 from jax.sharding import PartitionSpec as P
 
 PLAIN_HEAD_SIZE = 64
@@ -161,7 +165,488 @@
     return (mixer_out, expert_out)
 
 
+MESH = pl.DeviceIdType.MESH
+BF = jnp.bfloat16
+F32 = jnp.float32
+
+
+def dot(a, b):
+    return jnp.dot(a, b, preferred_element_type=F32)
+
+
+def fused_kernel(
+    n_z,
+    n_x,
+    q_ref,
+    lat_ref,
+    kr_ref,
+    lgain_ref,
+    tok_ref,
+    mgain_ref,
+    glog_ref,
+    ilog_ref,
+    pick_ref,
+    cos_ref,
+    sin_ref,
+    upw_hbm,
+    wout_hbm,
+    wg_hbm,
+    wu_hbm,
+    wd_hbm,
+    mix_ref,
+    exp_ref,
+    upw,
+    wout,
+    wg,
+    wu,
+    wd,
+    nrm,
+    dsend,
+    xb,
+    gate,
+    up,
+    hidden,
+    pa,
+    ra,
+    pb,
+    rb,
+    pc,
+    rc,
+    po,
+    rsend,
+    ret,
+    kv,
+    qt,
+    att,
+    mpart,
+    mrecv,
+    w_sem,
+    z_sem,
+    x_sem,
+    y_sem,
+    c_sem,
+    f_sem,
+    p_sem,
+    rb_sem,
+    ret_sem,
+    kz_sem,
+    kx_sem,
+    m_sem,
+):
+    ep = lax.axis_index("ep")
+    tp = lax.axis_index("tp")
+    z, x = ep // n_x, lax.rem(ep, n_x)
+    y, c = tp // 2, lax.rem(tp, 2)
+    ox = 1 - x
+    rows = tok_ref.shape[0]
+    cap = dsend.shape[1]
+    width = dsend.shape[2]
+    heads = qt.shape[1] // 128
+    other_x = (z * n_x + ox, tp)
+    core = tp + 1 - 2 * c
+    over = tp + 2 - 4 * y
+    diag = 3 - tp
+    to_core, to_y = (ep, core), (ep, over)
+
+    loads = []
+    for i, (a, b) in enumerate(
+        ((upw_hbm, upw), (wg_hbm.at[0], wg), (wu_hbm.at[0], wu), (wd_hbm.at[0], wd), (wout_hbm, wout))
+    ):
+        cp = pltpu.make_async_copy(a, b, w_sem.at[i])
+        cp.start()
+        loads.append(cp)
+
+    barrier = pltpu.get_barrier_semaphore()
+    n_ep = n_z * n_x
+    for d in range(1, n_ep):
+        pl.semaphore_signal(
+            barrier, inc=1, device_id=(lax.rem(ep + d, n_ep), tp), device_id_type=MESH
+        )
+    for d in range(1, 4):
+        pl.semaphore_signal(
+            barrier, inc=1, device_id=(ep, lax.rem(tp + d, 4)), device_id_type=MESH
+        )
+
+    pending = []
+
+    def send(src, dst, sem, device):
+        cp = pltpu.make_async_remote_copy(
+            src_ref=src,
+            dst_ref=dst,
+            send_sem=sem.at[0],
+            recv_sem=sem.at[1],
+            device_id=device,
+            device_id_type=MESH,
+        )
+        cp.start()
+        pending.append(cp)
+        return cp
+
+    values_f = tok_ref[...].astype(F32)
+    centered = values_f - jnp.mean(values_f, axis=-1, keepdims=True)
+    variance = jnp.mean(centered * centered, axis=-1, keepdims=True)
+    nrm[...] = (centered * lax.rsqrt(variance + 1e-05) * mgain_ref[...]).astype(BF)
+    mine = nrm[:, pl.ds(pl.multiple_of(tp * width, width), width)]
+    pick0 = pick_ref[:, 0:1]
+    pick1 = pick_ref[:, 1:2]
+    group = pick0 // n_x
+    group_one = (lax.broadcasted_iota(jnp.int32, (rows, 128), 1) == group).astype(F32)
+    below = (
+        lax.broadcasted_iota(jnp.int32, (rows, rows), 0)
+        > lax.broadcasted_iota(jnp.int32, (rows, rows), 1)
+    ).astype(F32)
+    counts = dot(below.astype(BF), group_one.astype(BF))
+    order_in = jnp.sum(counts * group_one, axis=1, keepdims=True)
+    slot = group.astype(F32) * float(cap) + order_in
+    slot_iota = lax.broadcasted_iota(jnp.int32, (rows, n_z * cap), 1).astype(F32)
+    table = (slot_iota == slot).astype(F32)
+    picked = dot(table.T.astype(BF), mine).astype(BF)
+    dsend[...] = picked.reshape(n_z, cap, width)
+    xb[tp, z, x] = dsend[z]
+
+    pl.semaphore_wait(barrier, n_ep + 2)
+
+    z_in = [None]
+    for d in range(1, n_z):
+        far = lax.rem(z + d, n_z)
+        z_in.append(send(dsend.at[far], xb.at[tp, z, x], z_sem.at[d], (far * n_x + x, tp)))
+
+    def block(d):
+        return lax.rem(z + n_z - d, n_z)
+
+    x_in, y_in, c_in = [], [], []
+
+    def relay_tp(d, side, xi):
+        ref = xb.at[tp, block(d), xi]
+        y_in.append(send(ref, ref, y_sem.at[d, side], to_y))
+        c_in.append(send(ref, ref, c_sem.at[d, side], to_core))
+
+    ref = xb.at[tp, z, x]
+    x_in.append(send(dsend.at[z], ref, x_sem.at[0], other_x))
+    relay_tp(0, 0, x)
+
+    latent = lat_ref[...].astype(F32)
+    normed_latent = (
+        latent
+        * lax.rsqrt(jnp.mean(latent * latent, axis=-1, keepdims=True) + 1e-06)
+        * lgain_ref[...]
+    ).astype(BF)
+    cosine, sine_part = cos_ref[...], sin_ref[...]
+    half = D_ROPE // 2
+    head_size = PLAIN_HEAD_SIZE + D_ROPE
+
+    def turn(values, n_heads, base, stride):
+        wide = n_heads * 128
+        src = lax.broadcasted_iota(jnp.int32, (values.shape[1], wide), 0)
+        lane = lax.broadcasted_iota(jnp.int32, (values.shape[1], wide), 1)
+        t = lax.rem(lane, 128)
+        want = (lane // 128) * stride + t - base
+        inside = (t >= base) & (t < head_size)
+        keep = ((src == want) & inside).astype(F32)
+        first = (t >= PLAIN_HEAD_SIZE) & (t < PLAIN_HEAD_SIZE + half)
+        second = (t >= PLAIN_HEAD_SIZE + half) & (t < head_size)
+        swap = ((src == want - half) & second).astype(F32) - ((src == want + half) & first).astype(
+            F32
+        )
+        a = dot(values, keep.astype(BF))
+        b = dot(values, swap.astype(BF))
+        cw = jnp.concatenate([cosine] * n_heads, axis=1)
+        sw = jnp.concatenate([sine_part] * n_heads, axis=1)
+        return (a * cw + b * sw).astype(BF)
+
+    loads[0].wait()
+    kv[z, x, :, 0 : heads * 128] = dot(normed_latent, upw[...]).astype(BF)
+    kv[z, x, :, heads * 128 :] = turn(kr_ref[...], 1, PLAIN_HEAD_SIZE, D_ROPE)
+    kz = [None]
+    own = kv.at[z, x]
+    for d in range(1, n_z):
+        far = lax.rem(z + d, n_z)
+        kz.append(send(own, own, kz_sem.at[d], (far * n_x + x, tp)))
+    kx = [send(own, own, kx_sem.at[0], other_x)]
+    qt[...] = turn(q_ref[...], heads, 0, head_size)
+
+    for d in range(1, n_z):
+        z_in[d].wait_recv()
+        ref = xb.at[tp, block(d), x]
+        x_in.append(send(ref, ref, x_sem.at[d], other_x))
+        relay_tp(d, 0, x)
+    for d in range(n_z):
+        x_in[d].wait_recv()
+        relay_tp(d, 1, ox)
+
+    tile = 256
+    inner = gate.shape[1]
+
+    def accumulate(q, fresh):
+        xin = xb[q].reshape(n_ep * cap, width)
+        weight_rows = pl.ds(pl.multiple_of(q * width, width), width)
+
+        def step(i, carry):
+            cols = pl.ds(pl.multiple_of(i * tile, tile), tile)
+            g = dot(xin, wg[weight_rows, cols])
+            u = dot(xin, wu[weight_rows, cols])
+            if fresh:
+                gate[:, cols] = g
+                up[:, cols] = u
+            else:
+                gate[:, cols] = gate[:, cols] + g
+                up[:, cols] = up[:, cols] + u
+            return carry
+
+        lax.fori_loop(0, inner // tile, step, 0)
+
+    loads[1].wait()
+    loads[2].wait()
+    accumulate(tp, True)
+    for d in range(1, n_z):
+        kz[d].wait_recv()
+        ref = kv.at[block(d), x]
+        kx.append(send(ref, ref, kx_sem.at[d], other_x))
+    for cp in c_in:
+        cp.wait_recv()
+    accumulate(core, False)
+    f_in = []
+    for side, xi in ((0, x), (1, ox)):
+        for d in range(n_z):
+            y_in[side * n_z + d].wait_recv()
+            ref = xb.at[over, block(d), xi]
+            f_in.append(send(ref, ref, f_sem.at[d, side], to_core))
+    accumulate(over, False)
+    for cp in f_in:
+        cp.wait_recv()
+
+    q = diag
+    xin = xb[q].reshape(n_ep * cap, width)
+    weight_rows = pl.ds(pl.multiple_of(q * width, width), width)
+
+    def last(i, carry):
+        cols = pl.ds(pl.multiple_of(i * tile, tile), tile)
+        g = gate[:, cols] + dot(xin, wg[weight_rows, cols])
+        u = up[:, cols] + dot(xin, wu[weight_rows, cols])
+        hidden[:, cols] = (g / (1.0 + jnp.exp(-g)) * u).astype(BF)
+        return carry
+
+    lax.fori_loop(0, inner // tile, last, 0)
+
+    loads[3].wait()
+    piece = n_x * cap
+
+    def down(q, put):
+        def step(i, carry):
+            block_rows = pl.ds(pl.multiple_of(i * piece, piece), piece)
+            cols = pl.ds(pl.multiple_of(q * width, width), width)
+            put(i, block_rows, dot(hidden[block_rows, :], wd[:, cols]).astype(BF))
+            return carry
+
+        lax.fori_loop(0, n_z, step, 0)
+
+    def put_pa(i, block_rows, value):
+        pa[i] = value
+
+    down(diag, put_pa)
+    a_in = send(pa, ra, p_sem.at[0], to_core)
+
+    def put_pb(i, block_rows, value):
+        pb[i] = value
+
+    down(over, put_pb)
+    a_in.wait_recv()
+    b_in = []
+    for d in range(1, n_z + 1):
+        s = block(d % n_z)
+        pb[s] = (pb[s].astype(F32) + ra[s].astype(F32)).astype(BF)
+        b_in.append(send(pb.at[s], rb.at[s], rb_sem.at[d - 1], to_y))
+
+    def put_pc(i, block_rows, value):
+        pc[i] = value
+
+    down(core, put_pc)
+    c2 = send(pc, rc, p_sem.at[1], to_core)
+
+    def put_po(i, block_rows, value):
+        po[i] = value
+
+    down(tp, put_po)
+
+    for cp in kx:
+        cp.wait_recv()
+    keys_all = n_ep * rows
+    tail = kv[:, :, :, heads * 128 :].reshape(keys_all, 128)
+    lane = lax.broadcasted_iota(jnp.int32, (keys_all, 128), 1)
+    q_seg = (ep * rows + lax.broadcasted_iota(jnp.int32, (rows, keys_all), 0)) // SEGMENT
+    k_seg = lax.broadcasted_iota(jnp.int32, (rows, keys_all), 1) // SEGMENT
+    allowed = q_seg >= k_seg
+    scale_factor = head_size ** (-0.5)
+    for h in range(heads):
+        kv_h = kv[:, :, :, h * 128 : (h + 1) * 128].reshape(keys_all, 128)
+        key_h = jnp.where(lane < PLAIN_HEAD_SIZE, kv_h, tail)
+        scores = lax.dot_general(
+            qt[:, h * 128 : (h + 1) * 128],
+            key_h,
+            (((1,), (1,)), ((), ())),
+            preferred_element_type=F32,
+        )
+        scores = jnp.where(allowed, scores * scale_factor, -jnp.inf)
+        weights = jnp.exp(scores - jnp.max(scores, axis=-1, keepdims=True))
+        denominator = jnp.sum(weights, axis=-1, keepdims=True)
+        done = dot(weights.astype(BF), kv_h) / denominator
+        att[:, h * VALUE_HEAD_SIZE : (h + 1) * VALUE_HEAD_SIZE] = done[:, PLAIN_HEAD_SIZE:].astype(BF)
+    loads[4].wait()
+    share = rows // 4
+    for j in range(4):
+        cols = slice(j * width, (j + 1) * width)
+        mpart[:, :, cols] = dot(att[...], wout[:, cols]).astype(BF).reshape(4, share, width)
+    m_in = []
+    for i, (q, dev) in enumerate(((core, to_core), (over, to_y), (diag, (ep, diag)))):
+        m_in.append(send(mpart.at[q], mrecv.at[i], m_sem.at[i], dev))
+
+    c2.wait_recv()
+    r_in = []
+    for d in range(1, n_z + 1):
+        dd = d % n_z
+        s = block(dd)
+        b_in[d - 1].wait_recv()
+        total = po[s].astype(F32) + rc[s].astype(F32) + rb[s].astype(F32)
+        rsend[s] = total.astype(BF).reshape(n_x, cap, width)
+        for side, xi in ((0, x), (1, ox)):
+            if dd == 0 and side == 0:
+                ret[x, z] = rsend[z, x]
+            else:
+                r_in.append(
+                    send(rsend.at[s, xi], ret.at[x, z], ret_sem.at[dd, side], (s * n_x + xi, tp))
+                )
+
+    for cp in m_in:
+        cp.wait_recv()
+    mix = mpart[tp].astype(F32)
+    for i in range(3):
+        mix = mix + mrecv[i].astype(F32)
+    mix_ref[...] = mix.astype(BF)
+
+    glog = glog_ref[...]
+    own_logit = jnp.sum(
+        jnp.where(lax.broadcasted_iota(jnp.int32, glog.shape, 1) == group, glog, 0.0),
+        axis=1,
+        keepdims=True,
+    )
+    group_share = 1.0 / jnp.sum(jnp.exp(glog - own_logit), axis=1, keepdims=True)
+    gap = ilog_ref[:, 0:1] - ilog_ref[:, 1:2]
+    w0 = group_share / (1.0 + jnp.exp(-gap))
+    w1 = group_share / (1.0 + jnp.exp(gap))
+
+    for cp in r_in:
+        cp.wait_recv()
+    table_b = table.astype(BF)
+    total = jnp.zeros((rows, width), F32)
+    for xi in range(n_x):
+        wx = jnp.where(lax.rem(pick0, n_x) == xi, w0, 0.0) + jnp.where(
+            lax.rem(pick1, n_x) == xi, w1, 0.0
+        )
+        total = total + wx * dot(table_b, ret[xi].reshape(n_z * cap, width))
+    exp_ref[...] = total.astype(BF)
+    for cp in pending:
+        cp.wait_send()
+
+
+def fused_device(n_z, n_x, *args):
+    (q, lat, kr, lgain, upw, wout, tok, mgain, glog, ilog, pick, wg, wu, wd) = args
+    rows = tok.shape[0]
+    model = tok.shape[1]
+    n_ep = n_z * n_x
+    cap = 4 * rows // n_ep
+    width = model // 4
+    inner = wg.shape[2]
+    heads = wout.shape[0] // VALUE_HEAD_SIZE
+    slots = n_ep * cap
+    lane = jnp.arange(128, dtype=jnp.int32)
+    half = D_ROPE // 2
+    j = (lane - PLAIN_HEAD_SIZE) % half
+    frequency = jnp.power(10000.0, -j.astype(F32) * 2.0 / D_ROPE)
+    positions = (lax.axis_index("ep") * rows + jnp.arange(rows, dtype=jnp.int32)).astype(F32)
+    angles = positions[:, None] * frequency[None, :]
+    turned = (lane >= PLAIN_HEAD_SIZE)[None, :]
+    cosine = jnp.where(turned, jnp.cos(angles), 1.0)
+    sine_part = jnp.where(turned, jnp.sin(angles), 0.0)
+    dma = pltpu.SemaphoreType.DMA
+    vmem = pltpu.VMEM
+    spec_v = pl.BlockSpec(memory_space=pltpu.VMEM)
+    spec_a = pl.BlockSpec(memory_space=pl.ANY)
+    return pl.pallas_call(
+        functools.partial(fused_kernel, n_z, n_x),
+        out_shape=(
+            jax.ShapeDtypeStruct((rows // 4, model), BF),
+            jax.ShapeDtypeStruct((rows, width), BF),
+        ),
+        in_specs=[spec_v] * 11 + [spec_a] * 5,
+        out_specs=(spec_v, spec_v),
+        scratch_shapes=[
+            vmem(upw.shape, BF),
+            vmem(wout.shape, BF),
+            vmem(wg.shape[1:], BF),
+            vmem(wu.shape[1:], BF),
+            vmem(wd.shape[1:], BF),
+            vmem((rows, model), BF),
+            vmem((n_z, cap, width), BF),
+            vmem((4, n_z, n_x, cap, width), BF),
+            vmem((slots, inner), F32),
+            vmem((slots, inner), F32),
+            vmem((slots, inner), BF),
+        ]
+        + [vmem((n_z, n_x * cap, width), BF)] * 7
+        + [
+            vmem((n_z, n_x, cap, width), BF),
+            vmem((n_x, n_z, cap, width), BF),
+            vmem((n_z, n_x, rows, heads * 128 + 128), BF),
+            vmem((rows, heads * 128), BF),
+            vmem((rows, heads * VALUE_HEAD_SIZE), BF),
+            vmem((4, rows // 4, model), BF),
+            vmem((3, rows // 4, model), BF),
+            dma((5,)),
+            dma((n_z, 2)),
+            dma((n_z, 2)),
+            dma((n_z, 2, 2)),
+            dma((n_z, 2, 2)),
+            dma((n_z, 2, 2)),
+            dma((2, 2)),
+            dma((n_z, 2)),
+            dma((n_z, 2, 2)),
+            dma((n_z, 2)),
+            dma((n_z, 2)),
+            dma((3, 2)),
+        ],
+        compiler_params=pltpu.CompilerParams(
+            collective_id=0, has_side_effects=True, vmem_limit_bytes=60 * 1024 * 1024
+        ),
+    )(
+        q,
+        lat,
+        kr,
+        lgain.reshape(1, -1),
+        tok,
+        mgain.reshape(1, -1),
+        glog,
+        ilog,
+        pick,
+        cosine,
+        sine_part,
+        upw,
+        wout,
+        wg,
+        wu,
+        wd,
+    )
+
+
 def solution(mesh):
+    n_ep = mesh.shape["ep"]
+    n_tp = mesh.shape["tp"]
+
+    def step(*args):
+        groups = args[8].shape[1]
+        if n_ep == 2 * groups and n_tp == 4:
+            return fused_device(groups, 2, *args)
+        return per_device(*args)
+
     in_specs = (
         P("ep", "tp"),
         P("ep", None),
@@ -180,5 +665,5 @@
     )
     out_specs = (P(("ep", "tp"), None), P("ep", "tp"))
     return jax.shard_map(
-        per_device, mesh=mesh, in_specs=in_specs, out_specs=out_specs, check_vma=False
-    )
+        step, mesh=mesh, in_specs=in_specs, out_specs=out_specs, check_vma=False
+    )

time: 174 us -> 66.9 us (0.38)
  waiting for transfers between devices: 79.7 us -> 0 us
  Pallas kernels: 0 us -> 55.9 us
  blocking collectives: 26.2 us -> 0 us
  matrix products: 15.6 us -> 0 us
  between operations: 15.8 us -> 0.66 us
  starting transfers between devices: 12.3 us -> 0 us
  other arithmetic: 10.8 us -> 0.98 us
  local copies, waits for them, and re-layouts: 12.7 us -> 8.78 us
    all_to_all x2 -> x0, waiting for transfers between devices: 71 us -> none  [the longest x1 58.2 us: per_device(): lax.all_to_all(outbound, 'ep', split_axis=0, concat_axis=0, tiled=True)]
    pallas_call x0 -> x1, Pallas kernels: none -> 55.9 us  [fused_device(): pl.pallas_call(functools.partial(fused_kernel, n_z, n_x), out_shape=(jax....]
    all_gather x1 -> x0, blocking collectives: 26.2 us -> none  [per_device(): lax.all_gather(k_turned, 'ep', axis=0, tiled=True)]
    dot_general x8 -> x0, matrix products: 15.6 us -> none  [the longest x1 4.66 us: per_device(): jnp.dot(flat_rows, w_gate[0], preferred_element_type=jnp.float32)]
    all_to_all x2 -> x0, starting transfers between devices: 12.2 us -> none  [the longest x1 7.41 us: per_device(): lax.all_to_all(outbound, 'ep', split_axis=0, concat_axis=0, tiled=True)]
    reduce_scatter x2 -> x0, waiting for transfers between devices: 8.62 us -> none  [the longest x1 8.59 us: per_device(): lax.psum_scatter(jnp.dot(attended, w_out, preferred_element_type=jnp.floa...]
    unnamed x22 -> x6, local copies, waits for them, and re-layouts: 1.9 us -> 8.78 us
    gather x2 -> x0, local copies, waits for them, and re-layouts: 4.45 us -> none  [the longest x1 3.29 us: per_device(): normed[slot_rows] * slot_filled[:, None]]
  transfers between devices with their start and end apart: 5 -> 0, of which waited for: 3 -> 0; matrix products, arithmetic and copies ran while one was open for 12% -> 0% of each run, Pallas kernels for 0% -> 0%
where the time goes in v1:
time: 66.9 us; the launch traced here: 66.3 us
  Pallas kernels  55.9 us (84%)
  local copies, waits for them, and re-layouts  8.78 us (13%)
  other arithmetic  0.98 us (1%)
    pallas_call x1, Pallas kernels, fused_device(): pl.pallas_call(functools.partial(fused_kernel, n_z, n_x), out_shape=(jax....  55.9 us
    unnamed x6, local copies, waits for them, and re-layouts  8.78 us

profile of v1, /device:TPU:0, one launch (start us, length us, event | category | flops | bytes accessed | tf_op | source)
XLA Modules:
  0.0 66.3 jit_solution(17419602636840252221)
XLA Ops:
  0.7 1.4 %copy.16.kr_ref = bf16[128,32]{1,0:T(8,128)(2,1)} copy(bf16[128,32]{0,1:T(8,128)(2,1)} %param.16) | data formatting | bytes 16384 | tf_op args[2]
  2.1 1.4 %copy.17.glog_ref = f32[128,4]{1,0:T(8,128)} copy(f32[128,4]{0,1:T(4,128)} %param.22) | data formatting | bytes 4096 | tf_op args[8]
  3.5 1.4 %copy.18.ilog_ref = f32[128,2]{1,0:T(8,128)} copy(f32[128,2]{0,1:T(2,128)} %param.23) | data formatting | bytes 2048 | tf_op args[9]
  4.9 1.4 %copy.19.pick_ref = s32[128,2]{1,0:T(8,128)} copy(s32[128,2]{0,1:T(2,128)} %param.24) | data formatting | bytes 2048 | tf_op args[10]
  6.3 1.0 %fusion.1 = (f32[128,128]{1,0:T(8,128)}, f32[128,128]{1,0:T(8,128)}) fusion(f32[128]{0:T(128)S(1)} %fusion.5, f32[128]{0:T(128)S(1)} %add_convert_fusion, pred[128]{0:T(512)(128)(4,1)S(1)} %iota_compare_fusion), kind=kLoop, calls=%fused_computation.3 | loop fusion | flops 49152 | bytes 132224 | tf_op jit(solution)/shard_map/jit(_where)/select_n | solution.py:569
  7.3 55.9 %shard_map.149 = (bf16[32,2048]{1,0:T(8,128)(2,1)}, bf16[128,512]{1,0:T(8,128)(2,1)}) custom-call(bf16[128,384]{1,0:T(8,128)(2,1)} %q_ref.1, bf16[128,512]{1,0:T(8,128)(2,1)} %lat_ref.1, bf16[128,32]{1,0:T(8,128)(2,1)} %copy.16.kr_ref, f32[1,512]{1,0:T(1,128)} %bitcast.3, bf16[128,2048]{1,0:T(8,128)(2,1)} %tok_ref.1, f32[1,2048]{1,0:T(1,128)} %bitcast.2, ...), custom_call_target="tpu_custom_call" | custom-call | tf_op jit(solution)/shard_map/pallas_call | solution.py:574
  63.2 1.6 %copy.22 = bf16[32,2048]{1,0:T(8,128)(2,1)} copy(bf16[32,2048]{1,0:T(8,128)(2,1)} %get-tuple-element.6) | data formatting | bytes 262144
  64.8 1.6 %copy.23 = bf16[128,512]{1,0:T(8,128)(2,1)} copy(bf16[128,512]{1,0:T(8,128)(2,1)} %get-tuple-element.7) | data formatting | bytes 262144
  (3 shorter events, 0.0 us)

commit v2 on v1

--- a/solution.py
+++ b/solution.py
@@ -232,6 +232,9 @@
     kz_sem,
     kx_sem,
     m_sem,
+    a_sem,
+    narrow,
+    mpair,
 ):
     ep = lax.axis_index("ep")
     tp = lax.axis_index("tp")
@@ -287,8 +290,15 @@
     variance = jnp.mean(centered * centered, axis=-1, keepdims=True)
     nrm[...] = (centered * lax.rsqrt(variance + 1e-05) * mgain_ref[...]).astype(BF)
     mine = nrm[:, pl.ds(pl.multiple_of(tp * width, width), width)]
-    pick0 = pick_ref[:, 0:1]
-    pick1 = pick_ref[:, 1:2]
+    narrow[...] = jnp.zeros_like(narrow)
+    n_groups = glog_ref.shape[0]
+    narrow[0:2, :] = pick_ref[...].astype(F32)
+    narrow[8:10, :] = ilog_ref[...]
+    narrow[16 : 16 + n_groups, :] = glog_ref[...]
+    narrow[32 : 32 + D_ROPE, :] = kr_ref[...].astype(F32)
+    tall = narrow[...].T
+    pick0 = tall[:, 0:1].astype(jnp.int32)
+    pick1 = tall[:, 1:2].astype(jnp.int32)
     group = pick0 // n_x
     group_one = (lax.broadcasted_iota(jnp.int32, (rows, 128), 1) == group).astype(F32)
     below = (
@@ -302,7 +312,15 @@
     table = (slot_iota == slot).astype(F32)
     picked = dot(table.T.astype(BF), mine).astype(BF)
     dsend[...] = picked.reshape(n_z, cap, width)
-    xb[tp, z, x] = dsend[z]
+    table_t = table.T.astype(BF)
+    own_slots = (
+        lax.broadcasted_iota(jnp.int32, (cap, n_z * cap), 0) + z * cap
+        == lax.broadcasted_iota(jnp.int32, (cap, n_z * cap), 1)
+    ).astype(F32).astype(BF)
+    own_table = dot(own_slots, table_t).astype(BF)
+    own_rows = dot(own_table, nrm[...]).astype(BF)
+    for j in range(4):
+        xb[j, z, x] = own_rows[:, j * width : (j + 1) * width]
 
     pl.semaphore_wait(barrier, n_ep + 2)
 
@@ -323,7 +341,6 @@
 
     ref = xb.at[tp, z, x]
     x_in.append(send(dsend.at[z], ref, x_sem.at[0], other_x))
-    relay_tp(0, 0, x)
 
     latent = lat_ref[...].astype(F32)
     normed_latent = (
@@ -356,13 +373,13 @@
 
     loads[0].wait()
     kv[z, x, :, 0 : heads * 128] = dot(normed_latent, upw[...]).astype(BF)
-    kv[z, x, :, heads * 128 :] = turn(kr_ref[...], 1, PLAIN_HEAD_SIZE, D_ROPE)
+    kv[z, x, :, heads * 128 :] = turn(tall[:, 32 : 32 + D_ROPE].astype(BF), 1, PLAIN_HEAD_SIZE, D_ROPE)
     kz = [None]
     own = kv.at[z, x]
     for d in range(1, n_z):
         far = lax.rem(z + d, n_z)
         kz.append(send(own, own, kz_sem.at[d], (far * n_x + x, tp)))
-    kx = [send(own, own, kx_sem.at[0], other_x)]
+    kx = []
     qt[...] = turn(q_ref[...], heads, 0, head_size)
 
     for d in range(1, n_z):
@@ -373,6 +390,8 @@
     for d in range(n_z):
         x_in[d].wait_recv()
         relay_tp(d, 1, ox)
+
+    kx.append(send(own, own, kx_sem.at[0], other_x))
 
     tile = 256
     inner = gate.shape[1]
@@ -406,11 +425,11 @@
         cp.wait_recv()
     accumulate(core, False)
     f_in = []
-    for side, xi in ((0, x), (1, ox)):
-        for d in range(n_z):
-            y_in[side * n_z + d].wait_recv()
-            ref = xb.at[over, block(d), xi]
-            f_in.append(send(ref, ref, f_sem.at[d, side], to_core))
+    stops = [(d, 0, x) for d in range(1, n_z)] + [(d, 1, ox) for d in range(n_z)]
+    for arrival, (d, side, xi) in zip(y_in, stops):
+        arrival.wait_recv()
+        ref = xb.at[over, block(d), xi]
+        f_in.append(send(ref, ref, f_sem.at[d, side], to_core))
     accumulate(over, False)
     for cp in f_in:
         cp.wait_recv()
@@ -440,22 +459,27 @@
 
         lax.fori_loop(0, n_z, step, 0)
 
-    def put_pa(i, block_rows, value):
-        pa[i] = value
-
-    down(diag, put_pa)
-    a_in = send(pa, ra, p_sem.at[0], to_core)
-
-    def put_pb(i, block_rows, value):
-        pb[i] = value
-
-    down(over, put_pb)
-    a_in.wait_recv()
-    b_in = []
+    def part(q, s):
+        cols = pl.ds(pl.multiple_of(q * width, width), width)
+        block_rows = pl.ds(pl.multiple_of(s * piece, piece), piece)
+        return dot(hidden[block_rows, :], wd[:, cols]).astype(BF)
+
+    a_in, b_in = [], []
+
+    def pass_on(d):
+        s = block(d % n_z)
+        a_in[d - 1].wait_recv()
+        pb[s] = (pb[s].astype(F32) + ra[s].astype(F32)).astype(BF)
+        b_in.append(send(pb.at[s], rb.at[s], rb_sem.at[d - 1], to_y))
+
     for d in range(1, n_z + 1):
         s = block(d % n_z)
-        pb[s] = (pb[s].astype(F32) + ra[s].astype(F32)).astype(BF)
-        b_in.append(send(pb.at[s], rb.at[s], rb_sem.at[d - 1], to_y))
+        pa[s] = part(diag, s)
+        a_in.append(send(pa.at[s], ra.at[s], a_sem.at[d - 1], to_core))
+        pb[s] = part(over, s)
+        if d > 1:
+            pass_on(d - 1)
+    pass_on(n_z)
 
     def put_pc(i, block_rows, value):
         pc[i] = value
@@ -497,8 +521,11 @@
         cols = slice(j * width, (j + 1) * width)
         mpart[:, :, cols] = dot(att[...], wout[:, cols]).astype(BF).reshape(4, share, width)
     m_in = []
-    for i, (q, dev) in enumerate(((core, to_core), (over, to_y), (diag, (ep, diag)))):
-        m_in.append(send(mpart.at[q], mrecv.at[i], m_sem.at[i], dev))
+    for i, q in enumerate((diag, core)):
+        m_in.append(send(mpart.at[q], mrecv.at[i], m_sem.at[i], to_core))
+    m_in[0].wait_recv()
+    mpair[...] = (mpart[over].astype(F32) + mrecv[0].astype(F32)).astype(BF)
+    m_in.append(send(mpair, mrecv.at[2], m_sem.at[2], to_y))
 
     c2.wait_recv()
     r_in = []
@@ -516,21 +543,21 @@
                     send(rsend.at[s, xi], ret.at[x, z], ret_sem.at[dd, side], (s * n_x + xi, tp))
                 )
 
-    for cp in m_in:
+    for cp in m_in[1:]:
         cp.wait_recv()
     mix = mpart[tp].astype(F32)
-    for i in range(3):
+    for i in range(1, 3):
         mix = mix + mrecv[i].astype(F32)
     mix_ref[...] = mix.astype(BF)
 
-    glog = glog_ref[...]
+    glog = tall[:, 16 : 16 + n_groups]
     own_logit = jnp.sum(
         jnp.where(lax.broadcasted_iota(jnp.int32, glog.shape, 1) == group, glog, 0.0),
         axis=1,
         keepdims=True,
     )
     group_share = 1.0 / jnp.sum(jnp.exp(glog - own_logit), axis=1, keepdims=True)
-    gap = ilog_ref[:, 0:1] - ilog_ref[:, 1:2]
+    gap = tall[:, 8:9] - tall[:, 9:10]
     w0 = group_share / (1.0 + jnp.exp(-gap))
     w1 = group_share / (1.0 + jnp.exp(gap))
 
@@ -612,7 +639,10 @@
             dma((n_z, 2, 2)),
             dma((n_z, 2)),
             dma((n_z, 2)),
-            dma((3, 2)),
+            dma((4, 2)),
+            dma((n_z, 2)),
+            vmem((128, rows), F32),
+            vmem((rows // 4, model), BF),
         ],
         compiler_params=pltpu.CompilerParams(
             collective_id=0, has_side_effects=True, vmem_limit_bytes=60 * 1024 * 1024
@@ -620,13 +650,13 @@
     )(
         q,
         lat,
-        kr,
+        kr.T,
         lgain.reshape(1, -1),
         tok,
         mgain.reshape(1, -1),
-        glog,
-        ilog,
-        pick,
+        glog.T,
+        ilog.T,
+        pick.T,
         cosine,
         sine_part,
         upw,

time: 66.9 us -> 62.3 us (0.931)
  local copies, waits for them, and re-layouts: 8.78 us -> 3.14 us
  Pallas kernels: 55.9 us -> 57.3 us
    unnamed x6 -> x2, local copies, waits for them, and re-layouts: 8.78 us -> 3.14 us
    pallas_call x1, Pallas kernels: 55.9 us -> 57.3 us  [fused_device(): pl.pallas_call(functools.partial(fused_kernel, n_z, n_x), out_shape=(jax....]
where the time goes in v2:
time: 62.3 us; the launch traced here: 62.1 us
  Pallas kernels  57.3 us (92%)
  local copies, waits for them, and re-layouts  3.14 us (5%)
  other arithmetic  1 us (2%)
  between operations  0.66 us (1%)
    pallas_call x1, Pallas kernels, fused_device(): pl.pallas_call(functools.partial(fused_kernel, n_z, n_x), out_shape=(jax....  57.3 us
    unnamed x2, local copies, waits for them, and re-layouts  3.14 us

profile of v2, /device:TPU:0, one launch (start us, length us, event | category | flops | bytes accessed | tf_op | source)
XLA Modules:
  0.0 62.1 jit_solution(2152075478505484861)
XLA Ops:
  0.7 1.0 %fusion.1 = (f32[128,128]{1,0:T(8,128)}, f32[128,128]{1,0:T(8,128)}) fusion(f32[128]{0:T(128)S(1)} %fusion.5, f32[128]{0:T(128)S(1)} %add_convert_fusion, pred[128]{0:T(512)(128)(4,1)S(1)} %iota_compare_fusion), kind=kLoop, calls=%fused_computation.3 | loop fusion | flops 49152 | bytes 132224 | tf_op jit(solution)/shard_map/jit(_where)/select_n | solution.py:596
  1.6 57.3 %shard_map.149 = (bf16[32,2048]{1,0:T(8,128)(2,1)}, bf16[128,512]{1,0:T(8,128)(2,1)}) custom-call(bf16[128,384]{1,0:T(8,128)(2,1)} %q_ref.1, bf16[128,512]{1,0:T(8,128)(2,1)} %lat_ref.1, bf16[32,128]{1,0:T(8,128)(2,1)} %bitcast.6, f32[1,512]{1,0:T(1,128)} %bitcast.8, bf16[128,2048]{1,0:T(8,128)(2,1)} %tok_ref.1, f32[1,2048]{1,0:T(1,128)} %bitcast.7, ...), custom_call_target="tpu_custom_call" | custom-call | tf_op jit(solution)/shard_map/pallas_call | solution.py:601
  59.0 1.6 %copy.18 = bf16[32,2048]{1,0:T(8,128)(2,1)} copy(bf16[32,2048]{1,0:T(8,128)(2,1)} %get-tuple-element.6) | data formatting | bytes 262144
  60.6 1.6 %copy.19 = bf16[128,512]{1,0:T(8,128)(2,1)} copy(bf16[128,512]{1,0:T(8,128)(2,1)} %get-tuple-element.7) | data formatting | bytes 262144
  (3 shorter events, 0.0 us)
